TPU v7x, 32 devices: a whole 2x2x4 slice. The times are simulated.
32 devices in a mesh: ep: 4 (over z), tp: 8 (over y, x, core).
Axes of the slice: x: 2, y: 2, z: 4, core: 2. Of those that a mesh axis runs over, the one named last changes fastest.
Arguments:
- tokens: bfloat16 [512, 2048], P('ep', 'tp'), may hold values from -6 to 6
- routes: int32 [512, 2], P('ep'), may hold values from 0 to 3, as said below
- route_weights: float32 [512, 2], P('ep'), may hold values from 0.1 to 1
- grad_out: bfloat16 [512, 2048], P('ep', 'tp'), may hold values from -6 to 6
- w_gate: bfloat16 [4, 2048, 2048], P('ep', 'tp'), may hold values from -0.125 to 0.125
- w_up: bfloat16 [4, 2048, 2048], P('ep', 'tp'), may hold values from -0.125 to 0.125
- w_down: bfloat16 [4, 2048, 2048], P('ep', 'tp')
Outputs:
- grad_tokens: bfloat16 [512, 2048], P('ep', 'tp')
- grad_route: float32 [512, 2], P('ep')
- grad_gate: float32 [4, 2048, 2048], P('ep', 'tp')
- grad_up: float32 [4, 2048, 2048], P('ep', 'tp')
- grad_down: float32 [4, 2048, 2048], P('ep', 'tp')
- gate_row_norms: float32 [4, 2048], P('ep')
- up_row_norms: float32 [4, 2048], P('ep')
- down_row_norms: float32 [4, 2048], P('ep', 'tp')
Inputs may be any that keep to these rules, and one draw needn't show every extreme that they name: `routes`: each token names two different experts of one group: group g holds experts g * 4 to g * 4 + 3. Among the 128 rows of one device along ep no expert is named more than 64 times, and in every draw some expert is named exactly 64 times by the rows of every device along ep.
All inputs are finite; a program needn't handle non-finite values.
Results may differ from a plain program's by a relative error of at most 0.017.
Values may be sent and summed in bfloat16 or wider, within the bound.
A program may use at most 64 MiB of HBM per device.

v0:
```python
import jax
import jax.numpy as jnp
from jax import lax
from jax.sharding import PartitionSpec as P


def silu_parts(pre_act):
    sigmoid_val = jax.nn.sigmoid(pre_act)
    return (pre_act * sigmoid_val, sigmoid_val * (1.0 + pre_act * (1.0 - sigmoid_val)))


def per_device(tokens, routes, route_weights, grad_out, w_gate, w_up, w_down):
    token_count, feature_dev = tokens.shape
    experts_dev, hidden_dev, model_width = w_gate.shape
    ep_size = lax.axis_size("ep")
    expert_total = experts_dev * ep_size
    capacity = min(3 * token_count // expert_total, token_count // 2)
    slot_count = expert_total * capacity
    row_count = ep_size * capacity
    flat_ids = routes.reshape(-1)
    pair_count = flat_ids.shape[0]
    one_hot = (flat_ids[:, None] == jnp.arange(expert_total, dtype=jnp.int32)[None, :]).astype(
        jnp.bfloat16
    )
    lower = (
        jnp.arange(pair_count, dtype=jnp.int32)[:, None]
        > jnp.arange(pair_count, dtype=jnp.int32)[None, :]
    ).astype(jnp.bfloat16)
    earlier = jnp.dot(lower, one_hot, preferred_element_type=jnp.float32)
    slot_ids = jnp.sum(earlier * one_hot.astype(jnp.float32), axis=1).astype(jnp.int32)
    position = flat_ids % experts_dev * row_count + flat_ids // experts_dev * capacity + slot_ids
    dispatch = (position[None, :] == jnp.arange(slot_count, dtype=jnp.int32)[:, None]).astype(
        jnp.bfloat16
    )
    weight_flat = route_weights.reshape(-1)
    token_rows = jnp.repeat(tokens, 2, axis=0)
    scaled = (weight_flat[:, None] * jnp.repeat(grad_out, 2, axis=0).astype(jnp.float32)).astype(
        jnp.bfloat16
    )
    send_shape = (experts_dev, ep_size, capacity, feature_dev)
    x_send = (
        jnp.dot(dispatch, token_rows, preferred_element_type=jnp.float32)
        .astype(jnp.bfloat16)
        .reshape(send_shape)
    )
    s_send = (
        jnp.dot(dispatch, scaled, preferred_element_type=jnp.float32)
        .astype(jnp.bfloat16)
        .reshape(send_shape)
    )
    x_recv, s_recv = (
        lax.all_to_all(x_send, "ep", split_axis=1, concat_axis=1, tiled=True),
        lax.all_to_all(s_send, "ep", split_axis=1, concat_axis=1, tiled=True),
    )
    x_full, s_full = (
        lax.all_gather(x_recv, "tp", axis=3, tiled=True),
        lax.all_gather(s_recv, "tp", axis=3, tiled=True),
    )
    x_rows = x_full.reshape(experts_dev, row_count, model_width)
    s_rows = s_full.reshape(experts_dev, row_count, model_width)
    gate = jnp.einsum("erd,efd->erf", x_rows, w_gate, preferred_element_type=jnp.float32)
    up = jnp.einsum("erd,efd->erf", x_rows, w_up, preferred_element_type=jnp.float32)
    dhid = jnp.einsum("erd,efd->erf", s_rows, w_down, preferred_element_type=jnp.float32)
    active, slope = silu_parts(gate)
    hidden = (active * up).astype(jnp.bfloat16)
    partial_value = jnp.sum(hidden.astype(jnp.float32) * dhid, axis=2)
    dgate = (dhid * up * slope).astype(jnp.bfloat16)
    dup = (dhid * active).astype(jnp.bfloat16)
    grad_gate = jnp.einsum("erf,erd->efd", dgate, x_rows, preferred_element_type=jnp.float32)
    grad_up = jnp.einsum("erf,erd->efd", dup, x_rows, preferred_element_type=jnp.float32)
    grad_down = jnp.einsum("erf,erd->efd", hidden, s_rows, preferred_element_type=jnp.float32)
    back_terms = jnp.einsum("erf,efd->erd", dgate, w_gate, preferred_element_type=jnp.float32)
    back_terms = back_terms + jnp.einsum(
        "erf,efd->erd", dup, w_up, preferred_element_type=jnp.float32
    )
    back_terms = back_terms.reshape(experts_dev, ep_size, capacity, model_width)
    gate_norms = jnp.sum(grad_gate * grad_gate, axis=1)
    up_norms = jnp.sum(grad_up * grad_up, axis=1)
    down_norms = jnp.sum(grad_down * grad_down, axis=2)
    partial_value, gate_norms, up_norms = lax.psum((partial_value, gate_norms, up_norms), "tp")
    partial_sent = partial_value.reshape(experts_dev, ep_size, capacity)
    dtok_mine = lax.psum_scatter(
        back_terms.astype(jnp.bfloat16), "tp", scatter_dimension=3, tiled=True
    ).astype(jnp.float32)
    returned, partial_back = (
        lax.all_to_all(
            dtok_mine.astype(jnp.bfloat16), "ep", split_axis=1, concat_axis=1, tiled=True
        ).astype(dtok_mine.dtype),
        lax.all_to_all(
            partial_sent.astype(jnp.bfloat16), "ep", split_axis=1, concat_axis=1, tiled=True
        ).astype(partial_sent.dtype),
    )
    slot_rows = jnp.take(returned.reshape(slot_count, feature_dev), position, axis=0)
    grad_tokens = jnp.sum(slot_rows.reshape(token_count, 2, feature_dev), axis=1).astype(
        jnp.bfloat16
    )
    slot_partial = jnp.take(partial_back.reshape(slot_count), position, axis=0)
    grad_route = (slot_partial / weight_flat).reshape(token_count, 2)
    return (
        grad_tokens,
        grad_route,
        grad_gate,
        grad_up,
        grad_down,
        gate_norms,
        up_norms,
        down_norms,
    )


def solution(mesh):
    in_specs = (
        P("ep", "tp"),
        P("ep", None),
        P("ep", None),
        P("ep", "tp"),
        P("ep", "tp", None),
        P("ep", "tp", None),
        P("ep", "tp", None),
    )
    out_specs = (
        P("ep", "tp"),
        P("ep", None),
        P("ep", "tp", None),
        P("ep", "tp", None),
        P("ep", "tp", None),
        P("ep", None),
        P("ep", None),
        P("ep", "tp"),
    )
    return jax.shard_map(
        per_device, mesh=mesh, in_specs=in_specs, out_specs=out_specs, check_vma=False
    )
```

profile of v0, /device:TPU:0, one launch (start us, length us, event | category | flops | bytes accessed | tf_op | source)
XLA Modules:
  0.0 136.7 jit_solution(6601070424293304525)
XLA Ops:
  7.2 0.0 copy-start
  7.2 0.0 copy-start.7
  7.2 0.0 copy-start.2
  7.2 0.0 all-gather.5.cloned.1.call-start
  7.2 1.0 broadcast_in_dim.29
  8.3 0.1 reshape.212
  8.4 0.8 copy.29
  9.1 0.1 reshape.208
  9.3 0.2 fusion.1
  9.5 0.2 convolution_convert_fusion
  9.7 12.3 %all_to_all.20 = bf16[1,4,64,256]{3,2,0,1:T(8,128)(2,1)} all-to-all(bf16[1,4,64,256]{3,2,0,1:T(8,128)(2,1)S(1)} %bitcast.61), channel_id=1, replica_groups=mesh['ep'=4,'tp'=8] {'ep'}, dimensions={1} | all-to-all | bytes 262144 | tf_op jit(solution)/shard_map/all_to_all | solution.py:52
  22.0 0.0 all-gather.5.cloned.1.call-update
  22.1 0.0 all-gather.3.cloned.1.call-start
  22.1 0.9 broadcast_in_dim.28
  23.0 0.2 convert_element_type.104
  23.2 0.0 copy-done.7
  23.2 0.1 copy.31
  23.3 0.1 mul.106
  23.5 0.3 convolution_convert_fusion.1
  23.7 9.0 %all_to_all.21 = bf16[1,4,64,256]{3,2,0,1:T(8,128)(2,1)} all-to-all(bf16[1,4,64,256]{3,2,0,1:T(8,128)(2,1)S(1)} %bitcast.60), channel_id=1, replica_groups=mesh['ep'=4,'tp'=8] {'ep'}, dimensions={1} | all-to-all | bytes 262144 | tf_op jit(solution)/shard_map/all_to_all | solution.py:53
  32.7 0.0 all-gather.3.cloned.1.call-update
  32.7 0.0 reduce-scatter.2.cloned.1.call-start
  32.8 12.0 %all-gather.5.cloned.1.call-done = bf16[1,4,64,2048]{3,2,0,1:T(8,128)(2,1)} async-done(((bf16[1,4,64,256]{3,2,0,1:T(8,128)(2,1)}), bf16[1,4,64,2048]{3,2,0,1:T(8,128)(2,1)}) %all-gather.5.cloned.1.call-update) | async-done | bytes 1048592 | tf_op jit(solution)/shard_map/all_gather | solution.py:56
  44.8 0.0 copy-start.1
  44.8 0.0 copy-done.2
  44.8 2.5 %fusion.7 = f32[256,256]{0,1:T(8,128)} fusion(bf16[256,2048]{1,0:T(8,128)(2,1)} %bitcast.50, bf16[1,256,2048]{2,1,0:T(8,128)(2,1)S(1)} %copy-done.2), kind=kOutput, calls=%fused_computation.16 | convolution fusion | flops 268435456 | bytes 2359296 | tf_op jit(solution)/shard_map/erd,efd->erf/dot_general | solution.py:62
  47.3 0.0 copy-done
  47.3 0.0 copy-done.1
  47.3 1.2 fusion.4
  48.5 21.7 %all-gather.3.cloned.1.call-done = bf16[1,4,64,2048]{3,2,0,1:T(8,128)(2,1)} async-done(((bf16[1,4,64,256]{3,2,0,1:T(8,128)(2,1)}), bf16[1,4,64,2048]{3,2,0,1:T(8,128)(2,1)}) %all-gather.3.cloned.1.call-update) | async-done | bytes 1048592 | tf_op jit(solution)/shard_map/all_gather | solution.py:57
  70.2 3.4 %multiply_reduce_fusion.3 = (f32[256]{0:T(256)}, bf16[256,256]{0,1:T(8,128)(2,1)}, bf16[256,256]{0,1:T(8,128)(2,1)S(1)}, bf16[256,256]{0,1:T(8,128)(2,1)S(1)}) fusion(f32[256,256]{0,1:T(8,128)} %fusion.7, f32[256,256]{0,1:T(8,128)} %fusion.4, bf16[256,2048]{1,0:T(8,128)(2,1)} %bitcast.58, bf16[1,256,2048]{2,1,0:T(8,128)(2,1)} %param.13), kind=kOutput, calls=%fused_computation.20 | convolution fusion | flops 269614848 | bytes 3015680 | tf_op jit(solution)/shard_map/erd,efd->erf/dot_general | solution.py:63
  73.5 0.5 fusion.2
  74.0 1.5 %fusion = bf16[256,2048]{1,0:T(8,128)(2,1)} fusion(f32[256,2048]{1,0:T(8,128)S(1)} %fusion.2, bf16[256,256]{0,1:T(8,128)(2,1)S(1)} %get-tuple-element.40, bf16[1,256,2048]{2,1,0:T(8,128)(2,1)S(1)} %copy-done.2), kind=kOutput, calls=%fused_computation.3 | convolution fusion | flops 269484032 | bytes 4325376 | tf_op jit(solution)/shard_map/erf,efd->erd/dot_general | solution.py:73
  75.5 0.0 reduce-scatter.2.cloned.1.call-update
  75.6 0.1 mul.115
  75.7 0.8 convert_element_type.102
  76.5 0.6 pad_clamp_fusion
  77.1 1.8 %multiply_reduce_fusion.2 = (f32[2048]{0:T(1024)S(1)}, f32[256,2048]{1,0:T(8,128)}) fusion(bf16[256,256]{0,1:T(8,128)(2,1)S(1)} %get-tuple-element.39, bf16[256,2048]{1,0:T(8,128)(2,1)S(1)} %bitcast.52), kind=kOutput, calls=%fused_computation.6 | convolution fusion | flops 269481984 | bytes 3284992 | tf_op jit(solution)/shard_map/erf,erd->efd/dot_general | solution.py:69
  78.8 0.0 copy-start.3
  78.8 0.0 copy-start.5
  78.8 1.8 %multiply_reduce_fusion.1 = (f32[2048]{0:T(1024)S(1)}, f32[256,2048]{1,0:T(8,128)}) fusion(bf16[256,256]{0,1:T(8,128)(2,1)S(1)} %get-tuple-element.40, bf16[256,2048]{1,0:T(8,128)(2,1)S(1)} %bitcast.53), kind=kOutput, calls=%fused_computation.5 | convolution fusion | flops 269481984 | bytes 3284992 | tf_op jit(solution)/shard_map/erf,erd->efd/dot_general | solution.py:70
  80.6 0.0 copy-start.6
  80.6 25.0 %all-reduce = (bf16[1,256]{1,0:T(2,128)(2,1)S(1)}, f32[1,2048]{1,0:T(1,128)}, f32[1,2048]{1,0:T(1,128)}) all-reduce(f32[1,256]{1,0:T(1,128)} %bitcast.67, f32[1,2048]{1,0:T(1,128)S(1)} %bitcast.62, f32[1,2048]{1,0:T(1,128)S(1)} %bitcast.63), channel_id=1, replica_groups=mesh['ep'=4,'tp'=8] {'tp'}, use_global_device_ids=true, to_apply=%region_4.5 | all-reduce | flops 4352 | bytes 34304 | tf_op jit(solution)/shard_map/psum | solution.py:80
  105.6 0.7 convert_element_type.118
  106.3 4.6 %all-to-all-start.3 = ((bf16[1,4,64]{2,0,1:T(2,128)(2,1)}), bf16[1,4,64]{2,0,1:T(2,128)(2,1)S(1)}, u32[]{:S(2)}, u32[]{:S(2)}) async-start(bf16[1,4,64]{2,0,1:T(2,128)(2,1)} %convert_element_type.118), calls=%async_computation.4 | async-start | bytes 4096 | tf_op jit(solution)/shard_map/all_to_all | solution.py:89
  110.9 0.0 copy-done.3
  110.9 0.0 copy-done.5
  110.9 0.0 copy-start.4
  110.9 2.3 %multiply_reduce_fusion = (f32[256]{0:T(256)}, f32[256,2048]{1,0:T(8,128)}) fusion(bf16[256,256]{0,1:T(8,128)(2,1)S(1)} %copy-done.5, bf16[256,2048]{1,0:T(8,128)(2,1)S(1)} %bitcast.59), kind=kOutput, calls=%fused_computation.4 | convolution fusion | flops 269483776 | bytes 3277824 | tf_op jit(solution)/shard_map/erf,erd->efd/dot_general | solution.py:71
  113.2 3.2 %all-to-all-done.3 = bf16[1,4,64]{2,0,1:T(2,128)(2,1)S(1)} async-done(((bf16[1,4,64]{2,0,1:T(2,128)(2,1)}), bf16[1,4,64]{2,0,1:T(2,128)(2,1)S(1)}, u32[]{:S(2)}, u32[]{:S(2)}) %all-to-all-start.3) | async-done | bytes 544 | tf_op jit(solution)/shard_map/all_to_all | solution.py:89
  116.5 0.1 reshape.224
  116.6 0.0 copy-done.6
  116.6 1.9 %gather_fusion.1 = f32[256]{0:T(256)S(1)} fusion(f32[256]{0:T(256)S(1)} %reshape.224, s32[1024]{0:T(1024)S(1)} %copy-done.6), kind=kCustom, calls=%fused_computation.1 | custom fusion | bytes 3072 | tf_op jit(solution)/shard_map/jit(_take)/gather | solution.py:97
  118.5 0.1 gather.15
  118.7 0.0 reduce-scatter.2.cloned.1.call-done
  118.7 3.3 %all-to-all-start.2 = ((bf16[1,4,64,256]{3,2,0,1:T(8,128)(2,1)}), bf16[1,4,64,256]{3,2,0,1:T(8,128)(2,1)S(1)}, u32[]{:S(2)}, u32[]{:S(2)}) async-start(bf16[1,4,64,256]{3,2,0,1:T(8,128)(2,1)} %reduce-scatter.2.cloned.1.call-done), calls=%async_computation.3 | async-start | bytes 262144 | tf_op jit(solution)/shard_map/all_to_all | solution.py:86
  122.0 0.0 copy-done.4
  122.1 0.6 copy.37
  122.7 5.2 %all-to-all-done.2 = bf16[1,4,64,256]{3,2,0,1:T(8,128)(2,1)S(1)} async-done(((bf16[1,4,64,256]{3,2,0,1:T(8,128)(2,1)}), bf16[1,4,64,256]{3,2,0,1:T(8,128)(2,1)S(1)}, u32[]{:S(2)}, u32[]{:S(2)}) %all-to-all-start.2) | async-done | bytes 131104 | tf_op jit(solution)/shard_map/all_to_all | solution.py:86
  127.9 1.0 gather_fusion
  128.9 0.1 gather.13
  129.1 1.1 select_reduce_fusion
  (8 shorter events, 0.1 us)
Async XLA Ops:
  7.2 40.1 %copy-start = (bf16[1,256,2048]{2,1,0:T(8,128)(2,1)S(1)}, bf16[1,256,2048]{2,1,0:T(8,128)(2,1)}, u32[]{:S(2)}) copy-start(bf16[1,256,2048]{2,1,0:T(8,128)(2,1)} %param.11) | copy-start | bytes 3145732
  7.2 16.0 %copy-start.7 = (f32[128,2]{0,1:T(2,128)S(1)}, f32[128,2]{0,1:T(2,128)}, u32[]{:S(2)}) copy-start(f32[128,2]{0,1:T(2,128)} %param.9) | copy-start | bytes 3076
  7.2 37.6 %copy-start.2 = (bf16[1,256,2048]{2,1,0:T(8,128)(2,1)S(1)}, bf16[1,256,2048]{2,1,0:T(8,128)(2,1)}, u32[]{:S(2)}) copy-start(bf16[1,256,2048]{2,1,0:T(8,128)(2,1)} %param.12) | copy-start | bytes 3145732
  7.2 37.6 %all-gather.5.cloned.1.call-start = ((), (), s32[]{:S(2)}) async-start(), calls=%async_computation.6 | async-start | bytes 1179648 | tf_op jit(solution)/shard_map/all_gather | solution.py:56
  22.1 48.1 %all-gather.3.cloned.1.call-start = ((), (), s32[]{:S(2)}) async-start(), calls=%async_computation.5 | async-start | bytes 1179648 | tf_op jit(solution)/shard_map/all_gather | solution.py:57
  32.7 85.9 %reduce-scatter.2.cloned.1.call-start = ((), (), s32[]{:S(2)}) async-start(), calls=%async_computation.7 | async-start | bytes 1179648 | tf_op jit(solution)/shard_map/reduce_scatter | solution.py:82
  44.8 2.5 %copy-start.1 = (bf16[1,4,64,2048]{3,2,0,1:T(8,128)(2,1)S(1)}, bf16[1,4,64,2048]{3,2,0,1:T(8,128)(2,1)}, u32[]{:S(2)}) copy-start(bf16[1,4,64,2048]{3,2,0,1:T(8,128)(2,1)} %all-gather.5.cloned.1.call-done) | copy-start | bytes 3145732
  78.8 32.0 %copy-start.3 = (bf16[1,4,64,2048]{3,2,0,1:T(8,128)(2,1)S(1)}, bf16[1,4,64,2048]{3,2,0,1:T(8,128)(2,1)}, u32[]{:S(2)}) copy-start(bf16[1,4,64,2048]{3,2,0,1:T(8,128)(2,1)} %all-gather.3.cloned.1.call-done) | copy-start | bytes 3145732
  78.8 32.0 %copy-start.5 = (bf16[256,256]{0,1:T(8,128)(2,1)S(1)}, bf16[256,256]{0,1:T(8,128)(2,1)}, u32[]{:S(2)}) copy-start(bf16[256,256]{0,1:T(8,128)(2,1)} %get-tuple-element.38) | copy-start | bytes 393220
  80.6 36.0 %copy-start.6 = (s32[1024]{0:T(1024)S(1)}, s32[1024]{0:T(1024)}, u32[]{:S(2)}) copy-start(s32[1024]{0:T(1024)} %pad_clamp_fusion) | copy-start | bytes 12292
  106.3 10.2 %all-to-all-start.3 = ((bf16[1,4,64]{2,0,1:T(2,128)(2,1)}), bf16[1,4,64]{2,0,1:T(2,128)(2,1)S(1)}, u32[]{:S(2)}, u32[]{:S(2)}) async-start(bf16[1,4,64]{2,0,1:T(2,128)(2,1)} %convert_element_type.118), calls=%async_computation.4 | async-start | bytes 4096 | tf_op jit(solution)/shard_map/all_to_all | solution.py:89
  110.9 11.1 %copy-start.4 = (s32[128,2]{1,0:T(8,128)S(1)}, s32[128,2]{1,0:T(8,128)}, u32[]{:S(2)}) copy-start(s32[128,2]{1,0:T(8,128)} %convert_element_type.102) | copy-start | bytes 3076
  118.7 9.2 %all-to-all-start.2 = ((bf16[1,4,64,256]{3,2,0,1:T(8,128)(2,1)}), bf16[1,4,64,256]{3,2,0,1:T(8,128)(2,1)S(1)}, u32[]{:S(2)}, u32[]{:S(2)}) async-start(bf16[1,4,64,256]{3,2,0,1:T(8,128)(2,1)} %reduce-scatter.2.cloned.1.call-done), calls=%async_computation.3 | async-start | bytes 262144 | tf_op jit(solution)/shard_map/all_to_all | solution.py:86
Sparse Core Ops, SparseCore 0:
  22.2 22.5 all-gather.4
  46.7 23.4 all-gather.2
  75.7 36.0 reduce-scatter.1
where the time goes:
time: 137 us
  blocking collectives  46.3 us (34%)
  waiting for transfers between devices  42.2 us (31%)
  matrix products  15.5 us (11%)
  between operations  13.9 us (10%)
  local copies, waits for them, and re-layouts  8.93 us (7%)
  starting transfers between devices  8.05 us (6%)
  other arithmetic  1.78 us (1%)
    psum x1, blocking collectives, per_device(): lax.psum((partial_value, gate_norms, up_norms), 'tp')  25 us
    all_gather x1, waiting for transfers between devices, per_device(): lax.all_gather(s_recv, 'tp', axis=3, tiled=True)  21.7 us
    all_to_all x1, blocking collectives, per_device(): lax.all_to_all(x_send, 'ep', split_axis=1, concat_axis=1, tiled=True)  12.3 us
    all_gather x1, waiting for transfers between devices, per_device(): lax.all_gather(x_recv, 'tp', axis=3, tiled=True)  12 us
    all_to_all x1, blocking collectives, per_device(): lax.all_to_all(s_send, 'ep', split_axis=1, concat_axis=1, tiled=True)  8.96 us
    all_to_all x1, waiting for transfers between devices, per_device(): lax.all_to_all(dtok_mine.astype(jnp.bfloat16), 'ep', split_axis=1, concat...  5.2 us
    all_to_all x1, starting transfers between devices, per_device(): lax.all_to_all(partial_sent.astype(jnp.bfloat16), 'ep', split_axis=1, con...  4.6 us
    dot_general x1, matrix products, per_device(): jnp.einsum('erd,efd->erf', s_rows, w_down, preferred_element_type=jnp.flo...  3.37 us
  transfers between devices with their start and end apart: 5, of which 4 were waited for; matrix products, arithmetic and copies ran while one was open for 12% of the time, Pallas kernels for 0%

commit v1 on v0

--- a/solution.py
+++ b/solution.py
@@ -1,7 +1,443 @@
+import functools
+
 import jax
 import jax.numpy as jnp
 from jax import lax
+from jax.experimental import pallas as pl
+from jax.experimental.pallas import tpu as pltpu
 from jax.sharding import PartitionSpec as P
+
+MESH = pl.DeviceIdType.MESH
+F32 = jnp.float32
+BF16 = jnp.bfloat16
+NT = (((1,), (1,)), ((), ()))
+VMEM = pl.BlockSpec(memory_space=pltpu.VMEM)
+ANY = pl.BlockSpec(memory_space=pl.ANY)
+
+
+def peers(j):
+    core, x, y = j % 2, (j // 2) % 2, j // 4
+    partner = j + 1 - 2 * core
+    xnb = j + 2 - 4 * x
+    ynb = j + 4 - 8 * y
+    diag = xnb + 4 - 8 * y
+    return partner, xnb, ynb, diag
+
+
+def routing(routes_ref):
+    token_count = routes_ref.shape[1]
+    r0, r1 = routes_ref[0:1, :], routes_ref[1:2, :]
+    eid = lax.broadcasted_iota(jnp.int32, (8, token_count), 0)
+    m0, m1 = eid == r0, eid == r1
+    m = jnp.logical_or(m0, m1)
+    upper = (
+        lax.broadcasted_iota(jnp.int32, (token_count, token_count), 0)
+        < lax.broadcasted_iota(jnp.int32, (token_count, token_count), 1)
+    )
+    earlier = jnp.dot(
+        jnp.where(m, 1.0, 0.0).astype(BF16),
+        jnp.where(upper, 1.0, 0.0).astype(BF16),
+        preferred_element_type=F32,
+    )
+    slot = jnp.where(m, earlier, -1.0)
+    return m0, m1, slot
+
+
+def slot_mask(slot, e, capacity):
+    token_count = slot.shape[1]
+    ids = lax.broadcasted_iota(jnp.int32, (capacity, token_count), 0).astype(F32)
+    return slot[e : e + 1, :] == ids
+
+
+def signal_all(barrier, devices):
+    for device in devices:
+        pl.semaphore_signal(barrier, inc=1, device_id=device, device_id_type=MESH)
+
+
+def remote(src, dst, send_sem, recv_sem, device):
+    return pltpu.make_async_remote_copy(
+        src_ref=src,
+        dst_ref=dst,
+        send_sem=send_sem,
+        recv_sem=recv_sem,
+        device_id=device,
+        device_id_type=MESH,
+    )
+
+
+def dispatch_kernel(
+    n_ep, capacity, routes_ref, weights_ref, tok_ref, go_ref, full_ref, send_buf, zs, zr, ts, tr
+):
+    i, j = lax.axis_index("ep"), lax.axis_index("tp")
+    width = tok_ref.shape[1]
+    partner, xnb, ynb, diag = peers(j)
+    barrier = pltpu.get_barrier_semaphore()
+    greet = [(lax.rem(i + d, n_ep), j) for d in range(1, n_ep)]
+    greet += [(i, t) for t in (partner, xnb, ynb, diag)]
+    signal_all(barrier, greet)
+
+    m0, m1, slot = routing(routes_ref)
+    weight = jnp.where(m0, weights_ref[0:1, :], 0.0) + jnp.where(m1, weights_ref[1:2, :], 0.0)
+    for e in range(n_ep):
+        mask = slot_mask(slot, e, capacity)
+        pick = jnp.where(mask, 1.0, 0.0).astype(BF16)
+        rows = jnp.dot(pick, tok_ref[...], preferred_element_type=F32)
+        grads = jnp.dot(pick, go_ref[...], preferred_element_type=F32)
+        scale = jnp.sum(jnp.where(mask, weight[e : e + 1, :], 0.0), axis=1, keepdims=True)
+        send_buf[e, 0] = rows.astype(BF16)
+        send_buf[e, 1] = (grads * scale).astype(BF16)
+
+    def area(src, col):
+        return full_ref.at[
+            :,
+            pl.ds(pl.multiple_of(src * capacity, capacity), capacity),
+            pl.ds(pl.multiple_of(col * width, width), width),
+        ]
+
+    area(i, j)[...] = send_buf[i]
+    pl.semaphore_wait(barrier, len(greet))
+
+    z_copies = {}
+    for d in [2, 1, 3]:
+        e = lax.rem(i + d, n_ep)
+        z_copies[d] = remote(send_buf.at[e], area(i, j), zs.at[d], zr.at[d], (e, j))
+        z_copies[d].start()
+
+    order = [0, 1, 3, 2]
+    copies = []
+    heard = {}
+    for step in range(len(order) + 1):
+        if step < len(order):
+            d = order[step]
+            src = lax.rem(i + n_ep - d, n_ep)
+            if d > 0:
+                z_copies[d].wait_recv()
+            mine = area(src, j) if d > 0 else send_buf.at[i]
+            for kind, target in enumerate((diag, xnb, ynb, partner)):
+                copy = remote(
+                    mine, area(src, j), ts.at[kind, d], tr.at[kind, d], (i, target)
+                )
+                copy.start()
+                copies.append(copy)
+                heard[kind, d] = copy
+        if step > 0:
+            d = order[step - 1]
+            src = lax.rem(i + n_ep - d, n_ep)
+            for kind, owner in ((1, xnb), (2, ynb), (0, diag)):
+                heard[kind, d].wait_recv()
+                got = area(src, owner)
+                copy = remote(got, got, ts.at[4 + kind, d], tr.at[4 + kind, d], (i, partner))
+                copy.start()
+                copies.append(copy)
+                heard[4 + kind, d] = copy
+    for d in order:
+        for kind in (3, 4, 5, 6):
+            heard[kind, d].wait_recv()
+    for d in range(1, n_ep):
+        z_copies[d].wait_send()
+    for copy in copies:
+        copy.wait_send()
+
+
+def expert_kernel(
+    n_ep, capacity, full_hbm, wg_hbm, wu_hbm, wd_hbm,
+    gg_hbm, gu_hbm, gd_hbm, back_ref, small_ref, dn_ref,
+    full, wg, wu, wd, gg, gu, gd, in_sem, out_sem,
+):
+    loads = []
+    for index, (src, dst) in enumerate(
+        ((full_hbm, full), (wg_hbm, wg), (wu_hbm, wu), (wd_hbm, wd))
+    ):
+        load = pltpu.make_async_copy(src, dst, in_sem.at[index])
+        load.start()
+        loads.append(load)
+    hidden_dev, model_width = wg.shape
+    loads[0].wait()
+    loads[1].wait()
+    x, s = full[0], full[1]
+    gate = lax.dot_general(x, wg[...], NT, preferred_element_type=F32)
+    loads[2].wait()
+    up = lax.dot_general(x, wu[...], NT, preferred_element_type=F32)
+    loads[3].wait()
+    dhid = lax.dot_general(s, wd[...], NT, preferred_element_type=F32)
+    sig = 1.0 / (1.0 + jnp.exp(-gate))
+    active = gate * sig
+    slope = sig * (1.0 + gate * (1.0 - sig))
+    hidden_f = (active * up).astype(BF16).astype(F32)
+    dgate_f = dhid * up * slope
+    dup_f = dhid * active
+    dgate, dup = dgate_f.astype(BF16), dup_f.astype(BF16)
+    route_terms = hidden_f * dhid
+    small_ref[...] = jnp.zeros_like(small_ref)
+    rows_norm = model_width // 128
+    for e in range(n_ep):
+        block = route_terms[e * capacity : (e + 1) * capacity, :]
+        small_ref[2 * rows_norm + e : 2 * rows_norm + e + 1, 0:capacity] = jnp.sum(
+            block.T, axis=0, keepdims=True
+        )
+    dgate_t = dgate_f.T.astype(BF16)
+    dup_t = dup_f.T.astype(BF16)
+    hidden_t = hidden_f.T.astype(BF16)
+    tile = 512
+    stores = []
+    down_sums = jnp.zeros((hidden_dev, 128), F32)
+    for n in range(model_width // tile):
+        cols = slice(n * tile, (n + 1) * tile)
+        for index, (lhs, rhs, buf, out) in enumerate(
+            ((dgate_t, 0, gg, gg_hbm), (dup_t, 0, gu, gu_hbm), (hidden_t, 1, gd, gd_hbm))
+        ):
+            grad = jnp.dot(lhs, full[rhs, :, cols], preferred_element_type=F32)
+            buf[:, cols] = grad
+            store = pltpu.make_async_copy(
+                buf.at[:, cols], out.at[:, cols], out_sem.at[index, n]
+            )
+            store.start()
+            stores.append(store)
+            square = grad * grad
+            if index < 2:
+                norm = jnp.sum(square, axis=0, keepdims=True)
+                for q in range(tile // 128):
+                    row = index * rows_norm + n * (tile // 128) + q
+                    small_ref[row : row + 1, :] = norm[:, q * 128 : (q + 1) * 128]
+            else:
+                for q in range(tile // 128):
+                    down_sums = down_sums + square[:, q * 128 : (q + 1) * 128]
+    dn_ref[...] = jnp.sum(down_sums.T, axis=0, keepdims=True)
+    for n in range(model_width // tile):
+        cols = slice(n * tile, (n + 1) * tile)
+        back_ref[:, cols] = (
+            jnp.dot(dgate, wg[:, cols], preferred_element_type=F32)
+            + jnp.dot(dup, wu[:, cols], preferred_element_type=F32)
+        ).astype(BF16)
+    for store in stores:
+        store.wait()
+
+
+def combine_kernel(
+    n_ep, n_tp, capacity, routes_ref, weights_ref, back_ref, small_ref,
+    gt_ref, gr_ref, gn_ref, un_ref,
+    pair_in, chip_sum, plane_in, z_out, z_in, small_in, route_out, route_in,
+    ps, pr, cs, cr, zs, zr, ss, sr, rs, rr,
+):
+    i, j = lax.axis_index("ep"), lax.axis_index("tp")
+    width = gt_ref.shape[1]
+    n_chip = n_tp // 2
+    core = j % 2
+    partner, xnb, ynb, diag = peers(j)
+    barrier = pltpu.get_barrier_semaphore()
+    greet = [(lax.rem(i + d, n_ep), j) for d in range(1, n_ep)]
+    greet += [(i, lax.rem(j + d, n_tp)) for d in range(1, n_tp)]
+    signal_all(barrier, greet)
+    m0, m1, slot = routing(routes_ref)
+    pl.semaphore_wait(barrier, len(greet))
+
+    order = [2, 1, 3, 0]
+
+    def rows_of(d):
+        e = lax.rem(i + d, n_ep)
+        return pl.ds(pl.multiple_of(e * capacity, capacity), capacity)
+
+    def cols_of(t):
+        return pl.ds(pl.multiple_of(t * width, width), width)
+
+    pair = {}
+    for d in order:
+        for q in range(n_chip):
+            copy = remote(
+                back_ref.at[rows_of(d), cols_of(2 * q + 1 - core)],
+                pair_in.at[d, q],
+                ps.at[d, q],
+                pr.at[d, q],
+                (i, partner),
+            )
+            copy.start()
+            pair[d, q] = copy
+    small = []
+    for d in range(1, n_tp):
+        copy = remote(
+            small_ref, small_in.at[d - 1], ss.at[d - 1], sr.at[d - 1], (i, lax.rem(j + d, n_tp))
+        )
+        copy.start()
+        small.append(copy)
+
+    plane = {}
+    for d in order:
+        for q in range(n_chip):
+            pair[d, q].wait_recv()
+            mine = back_ref[rows_of(d), cols_of(2 * q + core)].astype(F32)
+            chip_sum[d, q] = (mine + pair_in[d, q].astype(F32)).astype(BF16)
+        for kind, target in enumerate((diag, xnb, ynb)):
+            copy = remote(
+                chip_sum.at[d, target // 2],
+                plane_in.at[d, kind],
+                cs.at[d, kind],
+                cr.at[d, kind],
+                (i, target),
+            )
+            copy.start()
+            plane[d, kind] = copy
+
+    total = small_ref[...]
+    for copy in small:
+        copy.wait_recv()
+    for d in range(1, n_tp):
+        total = total + small_in[d - 1]
+    rows_norm = gn_ref.shape[1] // 128
+    for r in range(rows_norm):
+        gn_ref[:, r * 128 : (r + 1) * 128] = total[r : r + 1, :]
+        un_ref[:, r * 128 : (r + 1) * 128] = total[rows_norm + r : rows_norm + r + 1, :]
+    route_out[...] = total[2 * rows_norm : 2 * rows_norm + 8, :]
+    route_in[i] = total[2 * rows_norm : 2 * rows_norm + 8, :]
+    route = []
+    for d in range(1, n_ep):
+        copy = remote(
+            route_out, route_in.at[i], rs.at[d], rr.at[d], (lax.rem(i + d, n_ep), j)
+        )
+        copy.start()
+        route.append(copy)
+
+    z_copies = []
+    for d in order:
+        for kind in range(3):
+            plane[d, kind].wait_recv()
+        done = (
+            chip_sum[d, j // 2].astype(F32)
+            + plane_in[d, 0].astype(F32)
+            + plane_in[d, 1].astype(F32)
+            + plane_in[d, 2].astype(F32)
+        ).astype(BF16)
+        if d == 0:
+            z_in[i] = done
+        else:
+            z_out[d] = done
+            copy = remote(
+                z_out.at[d], z_in.at[i], zs.at[d], zr.at[d], (lax.rem(i + d, n_ep), j)
+            )
+            copy.start()
+            z_copies.append(copy)
+
+    for copy in route:
+        copy.wait_recv()
+    masks = []
+    back_route = []
+    for e in range(n_ep):
+        pick = jnp.where(slot_mask(slot, e, capacity), 1.0, 0.0)
+        masks.append(pick)
+        values = route_in[e, pl.ds(i, 1), :][:, 0:capacity]
+        back_route.append(
+            jnp.dot(
+                values, pick, preferred_element_type=F32, precision=lax.Precision.HIGHEST
+            )
+        )
+    for k, m in enumerate((m0, m1)):
+        value = jnp.zeros_like(back_route[0])
+        for e in range(n_ep):
+            value = value + jnp.where(m[e : e + 1, :], back_route[e], 0.0)
+        gr_ref[k : k + 1, :] = value / weights_ref[k : k + 1, :]
+
+    for copy in z_copies:
+        copy.wait_recv()
+    acc = jnp.zeros(gt_ref.shape, F32)
+    for e in range(n_ep):
+        acc = acc + jnp.dot(masks[e].T.astype(BF16), z_in[e], preferred_element_type=F32)
+    gt_ref[...] = acc.astype(BF16)
+    for copy in (*pair.values(), *small, *plane.values(), *route, *z_copies):
+        copy.wait_send()
+
+
+def per_device_kernels(tokens, routes, route_weights, grad_out, w_gate, w_up, w_down):
+    token_count, width = tokens.shape
+    _, hidden_dev, model_width = w_gate.shape
+    n_ep, n_tp = lax.axis_size("ep"), lax.axis_size("tp")
+    capacity = min(3 * token_count // n_ep, token_count // 2)
+    rows = n_ep * capacity
+    routes_t, weights_t = routes.T, route_weights.T
+    dma = pltpu.SemaphoreType.DMA
+    full = pl.pallas_call(
+        functools.partial(dispatch_kernel, n_ep, capacity),
+        name="dispatch",
+        out_shape=jax.ShapeDtypeStruct((2, rows, model_width), BF16),
+        in_specs=[VMEM] * 4,
+        out_specs=VMEM,
+        scratch_shapes=[
+            pltpu.VMEM((n_ep, 2, capacity, width), BF16),
+            dma((n_ep,)),
+            dma((n_ep,)),
+            dma((7, n_ep)),
+            dma((7, n_ep)),
+        ],
+        compiler_params=pltpu.CompilerParams(collective_id=0, has_side_effects=True),
+    )(routes_t, weights_t, tokens, grad_out)
+
+    small_rows = 2 * (model_width // 128) + 8
+    grad_shape = jax.ShapeDtypeStruct((hidden_dev, model_width), F32)
+    grad_gate, grad_up, grad_down, back, small, down_norms = pl.pallas_call(
+        functools.partial(expert_kernel, n_ep, capacity),
+        name="expert",
+        out_shape=(
+            grad_shape,
+            grad_shape,
+            grad_shape,
+            jax.ShapeDtypeStruct((rows, model_width), BF16),
+            jax.ShapeDtypeStruct((small_rows, 128), F32),
+            jax.ShapeDtypeStruct((1, hidden_dev), F32),
+        ),
+        in_specs=[ANY] * 4,
+        out_specs=(ANY, ANY, ANY, VMEM, VMEM, VMEM),
+        scratch_shapes=[
+            pltpu.VMEM((2, rows, model_width), BF16),
+            *[pltpu.VMEM((hidden_dev, model_width), BF16)] * 3,
+            *[pltpu.VMEM((hidden_dev, model_width), F32)] * 3,
+            dma((4,)),
+            dma((3, model_width // 512)),
+        ],
+    )(full, w_gate[0], w_up[0], w_down[0])
+
+    block = (capacity, width)
+    n_chip = n_tp // 2
+    grad_tokens, grad_route, gate_norms, up_norms = pl.pallas_call(
+        functools.partial(combine_kernel, n_ep, n_tp, capacity),
+        name="combine",
+        out_shape=(
+            jax.ShapeDtypeStruct((token_count, width), BF16),
+            jax.ShapeDtypeStruct((2, token_count), F32),
+            jax.ShapeDtypeStruct((1, model_width), F32),
+            jax.ShapeDtypeStruct((1, model_width), F32),
+        ),
+        in_specs=[VMEM] * 4,
+        out_specs=(VMEM,) * 4,
+        scratch_shapes=[
+            pltpu.VMEM((n_ep, n_chip, *block), BF16),
+            pltpu.VMEM((n_ep, n_chip, *block), BF16),
+            pltpu.VMEM((n_ep, 3, *block), BF16),
+            pltpu.VMEM((n_ep, *block), BF16),
+            pltpu.VMEM((n_ep, *block), BF16),
+            pltpu.VMEM((n_tp - 1, small_rows, 128), F32),
+            pltpu.VMEM((8, 128), F32),
+            pltpu.VMEM((n_ep, 8, 128), F32),
+            dma((n_ep, n_chip)),
+            dma((n_ep, n_chip)),
+            dma((n_ep, 3)),
+            dma((n_ep, 3)),
+            dma((n_ep,)),
+            dma((n_ep,)),
+            dma((n_tp - 1,)),
+            dma((n_tp - 1,)),
+            dma((n_ep,)),
+            dma((n_ep,)),
+        ],
+        compiler_params=pltpu.CompilerParams(collective_id=1, has_side_effects=True),
+    )(routes_t, weights_t, back, small)
+    return (
+        grad_tokens,
+        grad_route.T,
+        grad_gate[None],
+        grad_up[None],
+        grad_down[None],
+        gate_norms,
+        up_norms,
+        down_norms,
+    )
 
 
 def silu_parts(pre_act):
@@ -128,6 +564,7 @@
         P("ep", None),
         P("ep", "tp"),
     )
+    fits = mesh.shape["tp"] == 8 and mesh.shape["ep"] == 4
     return jax.shard_map(
-        per_device, mesh=mesh, in_specs=in_specs, out_specs=out_specs, check_vma=False
-    )
+        per_device_kernels if fits else per_device, mesh=mesh, in_specs=in_specs, out_specs=out_specs, check_vma=False
+    )

time: 137 us -> 55.9 us (0.41)
  Pallas kernels: 0 us -> 49.7 us
  blocking collectives: 46.3 us -> 0 us
  waiting for transfers between devices: 42.2 us -> 0 us
  matrix products: 15.5 us -> 0 us
  between operations: 13.9 us -> 0.66 us
  starting transfers between devices: 8.05 us -> 0 us
  local copies, waits for them, and re-layouts: 8.93 us -> 5.28 us
  other arithmetic: 1.78 us -> 0 us
    pallas_call x0 -> x3, Pallas kernels: none -> 49.7 us  [the longest x1 24.7 us: per_device_kernels(): pl.pallas_call(functools.partial(dispatch_kernel, n_ep, capacity), name='...]
    all_gather x2 -> x0, waiting for transfers between devices: 33.7 us -> none  [the longest x1 21.7 us: per_device(): lax.all_gather(s_recv, 'tp', axis=3, tiled=True)]
    psum x1 -> x0, blocking collectives: 25 us -> none  [per_device(): lax.psum((partial_value, gate_norms, up_norms), 'tp')]
    all_to_all x2 -> x0, blocking collectives: 21.3 us -> none  [the longest x1 12.3 us: per_device(): lax.all_to_all(x_send, 'ep', split_axis=1, concat_axis=1, tiled=True)]
    dot_general x11 -> x0, matrix products: 15.5 us -> none  [the longest x1 3.37 us: per_device(): jnp.einsum('erd,efd->erf', s_rows, w_down, preferred_element_type=jnp.flo...]
    all_to_all x2 -> x0, waiting for transfers between devices: 8.43 us -> none  [the longest x1 5.2 us: per_device(): lax.all_to_all(dtok_mine.astype(jnp.bfloat16), 'ep', split_axis=1, concat...]
    all_to_all x2 -> x0, starting transfers between devices: 7.93 us -> none  [the longest x1 4.6 us: per_device(): lax.all_to_all(partial_sent.astype(jnp.bfloat16), 'ep', split_axis=1, con...]
    unnamed x19 -> x4, local copies, waits for them, and re-layouts: 1.57 us -> 5.28 us
  transfers between devices with their start and end apart: 5 -> 0, of which waited for: 4 -> 0; matrix products, arithmetic and copies ran while one was open for 12% -> 0% of each run, Pallas kernels for 0% -> 0%
where the time goes in v1:
time: 55.9 us; the launch traced here: 55.6 us
  Pallas kernels  49.7 us (89%)
  local copies, waits for them, and re-layouts  5.28 us (9%)
  between operations  0.66 us (1%)
    pallas_call x1, Pallas kernels, per_device_kernels(): pl.pallas_call(functools.partial(dispatch_kernel, n_ep, capacity), name='...  24.7 us
    pallas_call x1, Pallas kernels, per_device_kernels(): pl.pallas_call(functools.partial(combine_kernel, n_ep, n_tp, capacity), n...  16.7 us
    pallas_call x1, Pallas kernels, per_device_kernels(): pl.pallas_call(functools.partial(expert_kernel, n_ep, capacity), name='ex...  8.26 us
    unnamed x4, local copies, waits for them, and re-layouts  5.28 us

profile of v1, /device:TPU:0, one launch (start us, length us, event | category | flops | bytes accessed | tf_op | source)
XLA Modules:
  0.0 55.6 jit_solution(16288439712222335961)
XLA Ops:
  0.6 24.7 %dispatch.1.full_hbm = bf16[2,256,2048]{2,1,0:T(8,128)(2,1)} custom-call(s32[2,128]{1,0:T(2,128)} %bitcast.12, f32[2,128]{1,0:T(2,128)} %bitcast.14, bf16[128,256]{1,0:T(8,128)(2,1)} %tok_ref.1, bf16[128,256]{1,0:T(8,128)(2,1)} %go_ref.1), custom_call_target="tpu_custom_call" | custom-call | tf_op jit(solution)/shard_map/dispatch/pallas_call | solution.py:356
  25.4 8.3 %expert.1 = (f32[256,2048]{1,0:T(8,128)}, f32[256,2048]{1,0:T(8,128)}, f32[256,2048]{1,0:T(8,128)}, bf16[256,2048]{1,0:T(8,128)(2,1)}, f32[40,128]{1,0:T(8,128)}, /*index=5*/f32[1,256]{1,0:T(1,128)}) custom-call(bf16[2,256,2048]{2,1,0:T(8,128)(2,1)} %dispatch.1.full_hbm, bf16[256,2048]{1,0:T(8,128)(2,1)} %bitcast.9, bf16[256,2048]{1,0:T(8,128)(2,1)} %bitcast.10, ...), custom_call_target="tpu_custom_call" | custom-call | tf_op jit(solution)/shard_map/expert/pallas_call | solution.py:374
  33.6 16.7 %combine.1 = (bf16[128,256]{1,0:T(8,128)(2,1)}, f32[2,128]{1,0:T(2,128)}, f32[1,2048]{1,0:T(1,128)}, f32[1,2048]{1,0:T(1,128)}) custom-call(s32[2,128]{1,0:T(2,128)} %bitcast.13, f32[2,128]{1,0:T(2,128)} %bitcast.15, bf16[256,2048]{1,0:T(8,128)(2,1)} %get-tuple-element.18.back_ref, f32[40,128]{1,0:T(8,128)} %get-tuple-element.19.small_ref), custom_call_target="tpu_custom_call" | custom-call | tf_op jit(solution)/shard_map/combine/pallas_call | solution.py:398
  50.3 1.5 %copy.19 = bf16[128,256]{1,0:T(8,128)(2,1)} copy(bf16[128,256]{1,0:T(8,128)(2,1)} %get-tuple-element.36) | data formatting | bytes 131072
  51.8 1.2 %copy.20 = f32[128,2]{0,1:T(2,128)} copy(f32[128,2]{0,1:T(2,128)} %bitcast.16) | data formatting | bytes 2048
  53.0 1.3 %copy.21 = f32[1,2048]{1,0:T(1,128)} copy(f32[1,2048]{1,0:T(1,128)} %get-tuple-element.41) | data formatting | bytes 16384
  54.3 1.3 %copy.22 = f32[1,2048]{1,0:T(1,128)} copy(f32[1,2048]{1,0:T(1,128)} %get-tuple-element.42) | data formatting | bytes 16384

commit v2 on v0

--- a/solution.py
+++ b/solution.py
@@ -1,7 +1,443 @@
+import functools
+
 import jax
 import jax.numpy as jnp
 from jax import lax
+from jax.experimental import pallas as pl
+from jax.experimental.pallas import tpu as pltpu
 from jax.sharding import PartitionSpec as P
+
+MESH = pl.DeviceIdType.MESH
+F32 = jnp.float32
+BF16 = jnp.bfloat16
+NT = (((1,), (1,)), ((), ()))
+VMEM = pl.BlockSpec(memory_space=pltpu.VMEM)
+ANY = pl.BlockSpec(memory_space=pl.ANY)
+
+
+def peers(j):
+    core, x, y = j % 2, (j // 2) % 2, j // 4
+    partner = j + 1 - 2 * core
+    xnb = j + 2 - 4 * x
+    ynb = j + 4 - 8 * y
+    diag = xnb + 4 - 8 * y
+    return partner, xnb, ynb, diag
+
+
+def routing(routes_ref):
+    token_count = routes_ref.shape[1]
+    r0, r1 = routes_ref[0:1, :], routes_ref[1:2, :]
+    eid = lax.broadcasted_iota(jnp.int32, (8, token_count), 0)
+    m0, m1 = eid == r0, eid == r1
+    m = jnp.logical_or(m0, m1)
+    upper = (
+        lax.broadcasted_iota(jnp.int32, (token_count, token_count), 0)
+        < lax.broadcasted_iota(jnp.int32, (token_count, token_count), 1)
+    )
+    earlier = jnp.dot(
+        jnp.where(m, 1.0, 0.0).astype(BF16),
+        jnp.where(upper, 1.0, 0.0).astype(BF16),
+        preferred_element_type=F32,
+    )
+    slot = jnp.where(m, earlier, -1.0)
+    return m0, m1, slot
+
+
+def slot_mask(slot, e, capacity):
+    token_count = slot.shape[1]
+    ids = lax.broadcasted_iota(jnp.int32, (capacity, token_count), 0).astype(F32)
+    return slot[e : e + 1, :] == ids
+
+
+def signal_all(barrier, devices):
+    for device in devices:
+        pl.semaphore_signal(barrier, inc=1, device_id=device, device_id_type=MESH)
+
+
+def remote(src, dst, send_sem, recv_sem, device):
+    return pltpu.make_async_remote_copy(
+        src_ref=src,
+        dst_ref=dst,
+        send_sem=send_sem,
+        recv_sem=recv_sem,
+        device_id=device,
+        device_id_type=MESH,
+    )
+
+
+def step_kernel(
+    n_ep, n_tp, capacity, routes_ref, weights_ref, tok_ref, go_ref, wg_hbm, wu_hbm, wd_hbm,
+    full_hbm, lhs_ref, z_in, route_in, norm_total,
+    full, send_buf, wg, wu, wd, back, pair_in, chip_sum, plane_in, z_out,
+    part_out, part_in, route_out, norm_out, norm_in,
+    in_sem, zs, zr, ts, tr, ps, pr, cs, cr, qs, qr, rs, rr, ns, nr, bs, br,
+):
+    i, j = lax.axis_index("ep"), lax.axis_index("tp")
+    width = tok_ref.shape[1]
+    model_width = wg.shape[1]
+    n_chip = n_tp // 2
+    core = j % 2
+    partner, xnb, ynb, diag = peers(j)
+    barrier = pltpu.get_barrier_semaphore()
+    greet = [(lax.rem(i + d, n_ep), j) for d in range(1, n_ep)]
+    greet += [(i, lax.rem(j + d, n_tp)) for d in range(1, n_tp)]
+    signal_all(barrier, greet)
+    loads = []
+    for index, (source, target) in enumerate(((wg_hbm, wg), (wu_hbm, wu), (wd_hbm, wd))):
+        load = pltpu.make_async_copy(source, target, in_sem.at[index])
+        load.start()
+        loads.append(load)
+
+    m0, m1, slot = routing(routes_ref)
+    weight = jnp.where(m0, weights_ref[0:1, :], 0.0) + jnp.where(m1, weights_ref[1:2, :], 0.0)
+    for e in range(n_ep):
+        mask = slot_mask(slot, e, capacity)
+        pick = jnp.where(mask, 1.0, 0.0).astype(BF16)
+        rows = jnp.dot(pick, tok_ref[...], preferred_element_type=F32)
+        grads = jnp.dot(pick, go_ref[...], preferred_element_type=F32)
+        scale = jnp.sum(jnp.where(mask, weight[e : e + 1, :], 0.0), axis=1, keepdims=True)
+        send_buf[e, 0] = rows.astype(BF16)
+        send_buf[e, 1] = (grads * scale).astype(BF16)
+
+    def rows_at(e):
+        return pl.ds(pl.multiple_of(e * capacity, capacity), capacity)
+
+    def cols_at(t):
+        return pl.ds(pl.multiple_of(t * width, width), width)
+
+    def area(src, col):
+        return full.at[:, rows_at(src), cols_at(col)]
+
+    area(i, j)[...] = send_buf[i]
+    pl.semaphore_wait(barrier, len(greet))
+
+    z_copies = {}
+    for d in [2, 1, 3]:
+        e = lax.rem(i + d, n_ep)
+        z_copies[d] = remote(send_buf.at[e], area(i, j), zs.at[d], zr.at[d], (e, j))
+        z_copies[d].start()
+
+    copies = []
+    heard = {}
+
+    def push(kind, d, source, target, device):
+        copy = remote(source, target, ts.at[kind, d], tr.at[kind, d], (i, device))
+        copy.start()
+        copies.append(copy)
+        heard[kind, d] = copy
+
+    order = [0, 1, 3, 2]
+    for step in range(len(order) + 2):
+        if step < len(order):
+            d = order[step]
+            src = lax.rem(i + n_ep - d, n_ep)
+            if d > 0:
+                z_copies[d].wait_recv()
+            mine = area(src, j) if d > 0 else send_buf.at[i]
+            push(0, d, mine, area(src, j), xnb)
+            push(1, d, mine, area(src, j), ynb)
+            push(4, d, mine, area(src, j), partner)
+        if 0 < step <= len(order):
+            d = order[step - 1]
+            src = lax.rem(i + n_ep - d, n_ep)
+            heard[0, d].wait_recv()
+            half = full.at[0, rows_at(src), cols_at(xnb)]
+            push(2, d, half, half, ynb)
+            push(5, d, area(src, xnb), area(src, xnb), partner)
+            heard[1, d].wait_recv()
+            half = full.at[1, rows_at(src), cols_at(ynb)]
+            push(3, d, half, half, xnb)
+            push(6, d, area(src, ynb), area(src, ynb), partner)
+        if step > 1:
+            d = order[step - 2]
+            src = lax.rem(i + n_ep - d, n_ep)
+            for kind in (0, 1):
+                heard[2 + kind, d].wait_recv()
+                half = full.at[kind, rows_at(src), cols_at(diag)]
+                push(7 + kind, d, half, half, partner)
+    for d in order:
+        for kind in (4, 5, 6, 7, 8):
+            heard[kind, d].wait_recv()
+
+    save = pltpu.make_async_copy(full, full_hbm, in_sem.at[3])
+    save.start()
+    for load in loads:
+        load.wait()
+    gate = lax.dot_general(full[0], wg[...], NT, preferred_element_type=F32)
+    up = lax.dot_general(full[0], wu[...], NT, preferred_element_type=F32)
+    dhid = lax.dot_general(full[1], wd[...], NT, preferred_element_type=F32)
+    sig = 1.0 / (1.0 + jnp.exp(-gate))
+    active = gate * sig
+    slope = sig * (1.0 + gate * (1.0 - sig))
+    hidden_f = (active * up).astype(BF16).astype(F32)
+    dgate_f = dhid * up * slope
+    dup_f = dhid * active
+    dgate, dup = dgate_f.astype(BF16), dup_f.astype(BF16)
+
+    ring = [2, 1, 3, 0]
+    pair = {}
+    for q in range(n_chip):
+        cols = slice(2 * q * width, 2 * (q + 1) * width)
+        back[:, cols] = (
+            jnp.dot(dgate, wg[:, cols], preferred_element_type=F32)
+            + jnp.dot(dup, wu[:, cols], preferred_element_type=F32)
+        ).astype(BF16)
+        for d in ring:
+            e = lax.rem(i + d, n_ep)
+            pair[d, q] = remote(
+                back.at[rows_at(e), cols_at(2 * q + 1 - core)],
+                pair_in.at[d, q],
+                ps.at[d, q],
+                pr.at[d, q],
+                (i, partner),
+            )
+            pair[d, q].start()
+
+    route_terms = hidden_f * dhid
+    part_out[...] = jnp.zeros_like(part_out)
+    for e in range(n_ep):
+        block = route_terms[e * capacity : (e + 1) * capacity, :]
+        part_out[e : e + 1, 0:capacity] = jnp.sum(block.T, axis=0, keepdims=True)
+    part = []
+    for d in range(1, n_tp):
+        copy = remote(
+            part_out, part_in.at[d - 1], qs.at[d - 1], qr.at[d - 1], (i, lax.rem(j + d, n_tp))
+        )
+        copy.start()
+        part.append(copy)
+
+    plane = {}
+    for d in ring:
+        e = lax.rem(i + d, n_ep)
+        for q in range(n_chip):
+            pair[d, q].wait_recv()
+            mine = back[rows_at(e), cols_at(2 * q + core)].astype(F32)
+            chip_sum[d, q] = (mine + pair_in[d, q].astype(F32)).astype(BF16)
+        for kind, target in enumerate((diag, xnb, ynb)):
+            plane[d, kind] = remote(
+                chip_sum.at[d, target // 2],
+                plane_in.at[d, kind],
+                cs.at[d, kind],
+                cr.at[d, kind],
+                (i, target),
+            )
+            plane[d, kind].start()
+
+    lhs_ref[0] = dgate_f.T.astype(BF16)
+    lhs_ref[1] = dup_f.T.astype(BF16)
+    lhs_ref[2] = hidden_f.T.astype(BF16)
+    rows_norm = model_width // 128
+    tile = 512
+    for index in range(2):
+        for n in range(model_width // tile):
+            cols = slice(n * tile, (n + 1) * tile)
+            grad = jnp.dot(lhs_ref[index], full[0, :, cols], preferred_element_type=F32)
+            norm = jnp.sum(grad * grad, axis=0, keepdims=True)
+            for q in range(tile // 128):
+                row = index * rows_norm + n * (tile // 128) + q
+                norm_out[row : row + 1, :] = norm[:, q * 128 : (q + 1) * 128]
+    norms = []
+    for d in range(1, n_tp):
+        copy = remote(
+            norm_out, norm_in.at[d - 1], ns.at[d - 1], nr.at[d - 1], (i, lax.rem(j + d, n_tp))
+        )
+        copy.start()
+        norms.append(copy)
+
+    for copy in part:
+        copy.wait_recv()
+    total = part_out[...]
+    for d in range(1, n_tp):
+        total = total + part_in[d - 1]
+    route_out[...] = total
+    route_in[i] = total
+    route = []
+    for d in range(1, n_ep):
+        copy = remote(
+            route_out, route_in.at[i], rs.at[d], rr.at[d], (lax.rem(i + d, n_ep), j)
+        )
+        copy.start()
+        route.append(copy)
+
+    returns = []
+    for d in ring:
+        for kind in range(3):
+            plane[d, kind].wait_recv()
+        done = (
+            chip_sum[d, j // 2].astype(F32)
+            + plane_in[d, 0].astype(F32)
+            + plane_in[d, 1].astype(F32)
+            + plane_in[d, 2].astype(F32)
+        ).astype(BF16)
+        if d == 0:
+            z_in[i] = done
+        else:
+            z_out[d] = done
+            copy = remote(
+                z_out.at[d], z_in.at[i], bs.at[d], br.at[d], (lax.rem(i + d, n_ep), j)
+            )
+            copy.start()
+            returns.append(copy)
+
+    for copy in norms:
+        copy.wait_recv()
+    total = norm_out[...]
+    for d in range(1, n_tp):
+        total = total + norm_in[d - 1]
+    norm_total[...] = total
+    for copy in (*route, *returns):
+        copy.wait_recv()
+    for copy in (
+        *z_copies.values(), *copies, *pair.values(), *part, *plane.values(),
+        *norms, *route, *returns,
+    ):
+        copy.wait_send()
+    save.wait()
+
+
+def finish_kernel(
+    n_ep, capacity, routes_ref, weights_ref, full_hbm, lhs_ref, z_in, route_in, norm_total,
+    gg_hbm, gu_hbm, gd_hbm, gt_ref, gr_ref, gn_ref, un_ref, dn_ref,
+    full, gg, gu, gd, in_sem, out_sem,
+):
+    loads = []
+    for index in range(2):
+        load = pltpu.make_async_copy(full_hbm.at[index], full.at[index], in_sem.at[index])
+        load.start()
+        loads.append(load)
+    _, hidden_dev, _ = lhs_ref.shape
+    model_width = full.shape[2]
+    tile = 512
+    stores = []
+    down_sums = jnp.zeros((hidden_dev, 128), F32)
+    for index, (rhs, buf, out) in enumerate(((0, gg, gg_hbm), (0, gu, gu_hbm), (1, gd, gd_hbm))):
+        if index != 1:
+            loads[rhs].wait()
+        for n in range(model_width // tile):
+            cols = slice(n * tile, (n + 1) * tile)
+            grad = jnp.dot(lhs_ref[index], full[rhs, :, cols], preferred_element_type=F32)
+            buf[:, cols] = grad
+            store = pltpu.make_async_copy(
+                buf.at[:, cols], out.at[:, cols], out_sem.at[index, n]
+            )
+            store.start()
+            stores.append(store)
+            if index == 2:
+                square = grad * grad
+                for q in range(tile // 128):
+                    down_sums = down_sums + square[:, q * 128 : (q + 1) * 128]
+    dn_ref[...] = jnp.sum(down_sums.T, axis=0, keepdims=True)
+    rows_norm = model_width // 128
+    for r in range(rows_norm):
+        gn_ref[:, r * 128 : (r + 1) * 128] = norm_total[r : r + 1, :]
+        un_ref[:, r * 128 : (r + 1) * 128] = norm_total[rows_norm + r : rows_norm + r + 1, :]
+
+    i = lax.axis_index("ep")
+    m0, m1, slot = routing(routes_ref)
+    acc = jnp.zeros(gt_ref.shape, F32)
+    back_route = []
+    for e in range(n_ep):
+        pick = jnp.where(slot_mask(slot, e, capacity), 1.0, 0.0)
+        acc = acc + jnp.dot(pick.T.astype(BF16), z_in[e], preferred_element_type=F32)
+        values = route_in[e, pl.ds(i, 1), :][:, 0:capacity]
+        back_route.append(
+            jnp.dot(
+                values, pick, preferred_element_type=F32, precision=lax.Precision.HIGHEST
+            )
+        )
+    gt_ref[...] = acc.astype(BF16)
+    for k, m in enumerate((m0, m1)):
+        value = jnp.zeros_like(back_route[0])
+        for e in range(n_ep):
+            value = value + jnp.where(m[e : e + 1, :], back_route[e], 0.0)
+        gr_ref[k : k + 1, :] = value / weights_ref[k : k + 1, :]
+    for store in stores:
+        store.wait()
+
+
+def per_device_kernels(tokens, routes, route_weights, grad_out, w_gate, w_up, w_down):
+    token_count, width = tokens.shape
+    _, hidden_dev, model_width = w_gate.shape
+    n_ep, n_tp = lax.axis_size("ep"), lax.axis_size("tp")
+    n_chip = n_tp // 2
+    capacity = min(3 * token_count // n_ep, token_count // 2)
+    rows = n_ep * capacity
+    block = (capacity, width)
+    norm_rows = 2 * (model_width // 128)
+    routes_t, weights_t = routes.T, route_weights.T
+    dma = pltpu.SemaphoreType.DMA
+    full, lhs, z_in, route_in, norm_total = pl.pallas_call(
+        functools.partial(step_kernel, n_ep, n_tp, capacity),
+        name="step",
+        out_shape=(
+            jax.ShapeDtypeStruct((2, rows, model_width), BF16),
+            jax.ShapeDtypeStruct((3, hidden_dev, rows), BF16),
+            jax.ShapeDtypeStruct((n_ep, *block), BF16),
+            jax.ShapeDtypeStruct((n_ep, 8, 128), F32),
+            jax.ShapeDtypeStruct((norm_rows, 128), F32),
+        ),
+        in_specs=[VMEM] * 4 + [ANY] * 3,
+        out_specs=(ANY, VMEM, VMEM, VMEM, VMEM),
+        scratch_shapes=[
+            pltpu.VMEM((2, rows, model_width), BF16),
+            pltpu.VMEM((n_ep, 2, *block), BF16),
+            *[pltpu.VMEM((hidden_dev, model_width), BF16)] * 3,
+            pltpu.VMEM((rows, model_width), BF16),
+            pltpu.VMEM((n_ep, n_chip, *block), BF16),
+            pltpu.VMEM((n_ep, n_chip, *block), BF16),
+            pltpu.VMEM((n_ep, 3, *block), BF16),
+            pltpu.VMEM((n_ep, *block), BF16),
+            pltpu.VMEM((8, 128), F32),
+            pltpu.VMEM((n_tp - 1, 8, 128), F32),
+            pltpu.VMEM((8, 128), F32),
+            pltpu.VMEM((norm_rows, 128), F32),
+            pltpu.VMEM((n_tp - 1, norm_rows, 128), F32),
+            dma((4,)),
+            *[dma((n_ep,))] * 2,
+            *[dma((9, n_ep))] * 2,
+            *[dma((n_ep, n_chip))] * 2,
+            *[dma((n_ep, 3))] * 2,
+            *[dma((n_tp - 1,))] * 2,
+            *[dma((n_ep,))] * 2,
+            *[dma((n_tp - 1,))] * 2,
+            *[dma((n_ep,))] * 2,
+        ],
+        compiler_params=pltpu.CompilerParams(collective_id=0, has_side_effects=True),
+    )(routes_t, weights_t, tokens, grad_out, w_gate[0], w_up[0], w_down[0])
+
+    grad_shape = jax.ShapeDtypeStruct((hidden_dev, model_width), F32)
+    norm_shape = jax.ShapeDtypeStruct((1, model_width), F32)
+    grad_gate, grad_up, grad_down, grad_tokens, grad_route, gate_norms, up_norms, down_norms = (
+        pl.pallas_call(
+            functools.partial(finish_kernel, n_ep, capacity),
+            name="finish",
+            out_shape=(
+                *[grad_shape] * 3,
+                jax.ShapeDtypeStruct((token_count, width), BF16),
+                jax.ShapeDtypeStruct((2, token_count), F32),
+                *[norm_shape] * 2,
+                jax.ShapeDtypeStruct((1, hidden_dev), F32),
+            ),
+            in_specs=[VMEM, VMEM, ANY, VMEM, VMEM, VMEM, VMEM],
+            out_specs=(*[ANY] * 3, *[VMEM] * 5),
+            scratch_shapes=[
+                pltpu.VMEM((2, rows, model_width), BF16),
+                *[pltpu.VMEM((hidden_dev, model_width), F32)] * 3,
+                dma((2,)),
+                dma((3, model_width // 512)),
+            ],
+        )(routes_t, weights_t, full, lhs, z_in, route_in, norm_total)
+    )
+    return (
+        grad_tokens,
+        grad_route.T,
+        grad_gate[None],
+        grad_up[None],
+        grad_down[None],
+        gate_norms,
+        up_norms,
+        down_norms,
+    )
 
 
 def silu_parts(pre_act):
@@ -128,6 +564,7 @@
         P("ep", None),
         P("ep", "tp"),
     )
+    fits = mesh.shape["tp"] == 8 and mesh.shape["ep"] == 4
     return jax.shard_map(
-        per_device, mesh=mesh, in_specs=in_specs, out_specs=out_specs, check_vma=False
-    )
+        per_device_kernels if fits else per_device, mesh=mesh, in_specs=in_specs, out_specs=out_specs, check_vma=False
+    )

time: 137 us -> 46.8 us (0.34)
  blocking collectives: 46.3 us -> 0 us
  Pallas kernels: 0 us -> 45.9 us
  waiting for transfers between devices: 42.2 us -> 0 us
  matrix products: 15.5 us -> 0 us
  between operations: 13.9 us -> 0.64 us
  local copies, waits for them, and re-layouts: 8.93 us -> 0 us
  starting transfers between devices: 8.05 us -> 0 us
  other arithmetic: 1.78 us -> 0 us
    pallas_call x0 -> x2, Pallas kernels: none -> 45.9 us  [the longest x1 39.9 us: per_device_kernels(): pl.pallas_call(functools.partial(step_kernel, n_ep, n_tp, capacity), name...]
    all_gather x2 -> x0, waiting for transfers between devices: 33.7 us -> none  [the longest x1 21.7 us: per_device(): lax.all_gather(s_recv, 'tp', axis=3, tiled=True)]
    psum x1 -> x0, blocking collectives: 25 us -> none  [per_device(): lax.psum((partial_value, gate_norms, up_norms), 'tp')]
    all_to_all x2 -> x0, blocking collectives: 21.3 us -> none  [the longest x1 12.3 us: per_device(): lax.all_to_all(x_send, 'ep', split_axis=1, concat_axis=1, tiled=True)]
    dot_general x11 -> x0, matrix products: 15.5 us -> none  [the longest x1 3.37 us: per_device(): jnp.einsum('erd,efd->erf', s_rows, w_down, preferred_element_type=jnp.flo...]
    all_to_all x2 -> x0, waiting for transfers between devices: 8.43 us -> none  [the longest x1 5.2 us: per_device(): lax.all_to_all(dtok_mine.astype(jnp.bfloat16), 'ep', split_axis=1, concat...]
    all_to_all x2 -> x0, starting transfers between devices: 7.93 us -> none  [the longest x1 4.6 us: per_device(): lax.all_to_all(partial_sent.astype(jnp.bfloat16), 'ep', split_axis=1, con...]
    gather x4 -> x0, local copies, waits for them, and re-layouts: 3.19 us -> none  [the longest x2 2.08 us: per_device(): slot_partial = jnp.take(partial_back.reshape(slot_count), position, axis=0)]
  transfers between devices with their start and end apart: 5 -> 0, of which waited for: 4 -> 0; matrix products, arithmetic and copies ran while one was open for 12% -> 0% of each run, Pallas kernels for 0% -> 0%
where the time goes in v2:
time: 46.8 us; the launch traced here: 46.5 us
  Pallas kernels  45.9 us (98%)
  between operations  0.64 us (1%)
    pallas_call x1, Pallas kernels, per_device_kernels(): pl.pallas_call(functools.partial(step_kernel, n_ep, n_tp, capacity), name...  39.9 us
    pallas_call x1, Pallas kernels, per_device_kernels(): pl.pallas_call(functools.partial(finish_kernel, n_ep, capacity), name='fi...  5.97 us

profile of v2, /device:TPU:0, one launch (start us, length us, event | category | flops | bytes accessed | tf_op | source)
XLA Modules:
  0.0 46.5 jit_solution(14182939833730279150)
XLA Ops:
  0.6 39.9 %step.1 = (bf16[2,256,2048]{2,1,0:T(8,128)(2,1)}, bf16[3,256,256]{2,1,0:T(8,128)(2,1)}, bf16[4,64,256]{2,1,0:T(8,128)(2,1)}, f32[4,8,128]{2,1,0:T(8,128)}, f32[32,128]{1,0:T(8,128)}) custom-call(s32[2,128]{1,0:T(2,128)} %bitcast.12, f32[2,128]{1,0:T(2,128)} %bitcast.14, bf16[128,256]{1,0:T(8,128)(2,1)} %tok_ref.1, bf16[128,256]{1,0:T(8,128)(2,1)} %go_ref.1, ...), custom_call_target="tpu_custom_call" | custom-call | tf_op jit(solution)/shard_map/step/pallas_call | solution.py:369
  40.6 6.0 %finish.1 = (f32[256,2048]{1,0:T(8,128)}, f32[256,2048]{1,0:T(8,128)}, f32[256,2048]{1,0:T(8,128)}, bf16[128,256]{1,0:T(8,128)(2,1)}, f32[2,128]{1,0:T(2,128)}, ...) custom-call(s32[2,128]{1,0:T(2,128)} %bitcast.13, f32[2,128]{1,0:T(2,128)} %bitcast.15, ...), custom_call_target="tpu_custom_call" | custom-call | tf_op jit(solution)/shard_map/finish/pallas_call | solution.py:411

commit v3 on v2

--- a/solution.py
+++ b/solution.py
@@ -112,7 +112,7 @@
     pl.semaphore_wait(barrier, len(greet))
 
     z_copies = {}
-    for d in [2, 1, 3]:
+    for d in [1, 3, 2]:
         e = lax.rem(i + d, n_ep)
         z_copies[d] = remote(send_buf.at[e], area(i, j), zs.at[d], zr.at[d], (e, j))
         z_copies[d].start()

time: 46.8 us -> 45.5 us (0.972)
  Pallas kernels: 45.9 us -> 44.6 us
    pallas_call x1, Pallas kernels: 39.9 us -> 38.7 us  [per_device_kernels(): pl.pallas_call(functools.partial(step_kernel, n_ep, n_tp, capacity), name...]
where the time goes in v3:
time: 45.5 us; the launch traced here: 45.3 us
  Pallas kernels  44.6 us (98%)
  between operations  0.64 us (1%)
    pallas_call x1, Pallas kernels, per_device_kernels(): pl.pallas_call(functools.partial(step_kernel, n_ep, n_tp, capacity), name...  38.7 us
    pallas_call x1, Pallas kernels, per_device_kernels(): pl.pallas_call(functools.partial(finish_kernel, n_ep, capacity), name='fi...  5.97 us

profile of v3, /device:TPU:0, one launch (start us, length us, event | category | flops | bytes accessed | tf_op | source)
XLA Modules:
  0.0 45.3 jit_solution(14958629739026141783)
XLA Ops:
  0.6 38.7 %step.1 = (bf16[2,256,2048]{2,1,0:T(8,128)(2,1)}, bf16[3,256,256]{2,1,0:T(8,128)(2,1)}, bf16[4,64,256]{2,1,0:T(8,128)(2,1)}, f32[4,8,128]{2,1,0:T(8,128)}, f32[32,128]{1,0:T(8,128)}) custom-call(s32[2,128]{1,0:T(2,128)} %bitcast.12, f32[2,128]{1,0:T(2,128)} %bitcast.14, bf16[128,256]{1,0:T(8,128)(2,1)} %tok_ref.1, bf16[128,256]{1,0:T(8,128)(2,1)} %go_ref.1, ...), custom_call_target="tpu_custom_call" | custom-call | tf_op jit(solution)/shard_map/step/pallas_call | solution.py:369
  39.3 6.0 %finish.1 = (f32[256,2048]{1,0:T(8,128)}, f32[256,2048]{1,0:T(8,128)}, f32[256,2048]{1,0:T(8,128)}, bf16[128,256]{1,0:T(8,128)(2,1)}, f32[2,128]{1,0:T(2,128)}, ...) custom-call(s32[2,128]{1,0:T(2,128)} %bitcast.13, f32[2,128]{1,0:T(2,128)} %bitcast.15, ...), custom_call_target="tpu_custom_call" | custom-call | tf_op jit(solution)/shard_map/finish/pallas_call | solution.py:411
